TPU v7x, 32 devices: a whole 2x2x4 slice. The times are simulated.
32 devices in a mesh: sp: 8 (over z, y), dp: 4 (over x, core).
Axes of the slice: x: 2, y: 2, z: 4, core: 2. Of those that a mesh axis runs over, the one named last changes fastest.
Arguments:
- tokens: bfloat16 [4, 2560, 2048], P('dp', 'sp'), may hold values from -6 to 6
- w_query: bfloat16 [2048, 1024], P('dp', 'sp'), may hold values from -0.125 to 0.125
- w_key: bfloat16 [2048, 1024], P('dp', 'sp'), may hold values from -0.125 to 0.125
- w_value: bfloat16 [2048, 1024], P('dp', 'sp'), may hold values from -0.125 to 0.125
- w_output: bfloat16 [1024, 2048], P('sp', 'dp'), may hold values from -0.1875 to 0.1875
- qk_gain: float32 [2, 64], replicated, may hold values from 0.4 to 7
- decay_sums: float32 [4, 16, 2560], P('dp', 'sp'), may hold values from -512 to 0, as said below
Outputs:
- layer_out: bfloat16 [4, 2560, 2048], P('dp', 'sp')
Inputs may be any that keep to these rules, and one draw needn't show every extreme that they name: `decay_sums`: each row is non-increasing along positions.
All inputs are finite; a program needn't handle non-finite values.
Results may differ from a plain program's by a relative error of at most 0.0075.
The roundings to bfloat16 on the way count: a program that leaves them out, or rounds other values in their place, can miss the bound.
Values may be sent and summed in bfloat16 or wider, within the bound.
A program may use at most 128 MiB of HBM per device.

v0:
```python
import jax
import jax.numpy as jnp
from jax import lax
from jax.sharding import PartitionSpec as P


def normalize(values):
    values = values.astype(jnp.float32)
    return values * lax.rsqrt(jnp.mean(values * values, axis=-1, keepdims=True) + 1e-06)


def attend(query_unit, key_unit, value_rows, decay_rows):
    length = query_unit.shape[0]
    groups = query_unit.shape[1]
    width = query_unit.shape[2]
    block = min(512, length)

    def one_block(index):
        start = index * block
        query_block = lax.dynamic_slice_in_dim(query_unit, start, block, 0)
        decay_block = lax.dynamic_slice_in_dim(decay_rows, start, block, 1)
        query_place = start + jnp.arange(block, dtype=jnp.int32)

        def fill(column, buffer):
            key_start = column * block
            key_block = lax.dynamic_slice_in_dim(key_unit, key_start, block, 0)
            decay_keys = lax.dynamic_slice_in_dim(decay_rows, key_start, block, 1)
            scores = jnp.einsum(
                "qhd,khd->hqk", query_block, key_block, preferred_element_type=jnp.float32
            )
            scores = scores + decay_block[:, :, None] - decay_keys[:, None, :]
            key_place = key_start + jnp.arange(block, dtype=jnp.int32)
            scores = jnp.where(
                key_place[None, None, :] <= query_place[None, :, None], scores, -jnp.inf
            )
            return lax.dynamic_update_slice_in_dim(buffer, scores, key_start, 2)

        empty = jnp.full((groups, block, length), -jnp.inf, jnp.float32)
        scores = lax.fori_loop(0, index + 1, fill, empty)
        peak = jnp.max(scores, axis=-1, keepdims=True)
        weights = jnp.exp(scores - peak)
        probs = (weights / jnp.sum(weights, axis=-1, keepdims=True)).astype(jnp.bfloat16)

        def gather_values(column, running):
            key_start = column * block
            prob_block = lax.dynamic_slice_in_dim(probs, key_start, block, 2)
            value_block = lax.dynamic_slice_in_dim(value_rows, key_start, block, 0)
            return running + jnp.einsum(
                "hqk,khd->qhd", prob_block, value_block, preferred_element_type=jnp.float32
            )

        zeros = jnp.zeros((block, groups, width), jnp.float32)
        return lax.fori_loop(0, index + 1, gather_values, zeros)

    blocks = lax.map(one_block, jnp.arange(length // block, dtype=jnp.int32))
    return blocks.reshape(length, groups, width)


def on_device(tokens, w_query, w_key, w_value, w_output, qk_gain, decay_sums):
    own_rows = tokens[0]
    decay_rows = decay_sums[0]
    head_group = decay_rows.shape[0]
    head_dim = qk_gain.shape[1]
    stacked = jnp.stack((w_query, w_key, w_value))
    columns, out_columns = (
        lax.all_gather(stacked, "dp", axis=1, tiled=True),
        lax.all_gather(w_output, "dp", axis=1, tiled=True),
    )
    whole = lax.all_gather(own_rows, "sp", axis=0, tiled=True)
    triple = jnp.einsum("td,kdc->ktc", whole, columns, preferred_element_type=jnp.float32).astype(
        jnp.bfloat16
    )
    length = triple.shape[1]
    grouped = triple.reshape(3, length, head_group, head_dim)
    query_unit = (normalize(grouped[0]) * qk_gain[0] * head_dim ** (-0.5)).astype(jnp.bfloat16)
    key_unit = (normalize(grouped[1]) * qk_gain[1]).astype(jnp.bfloat16)
    attended = attend(query_unit, key_unit, grouped[2], decay_rows)
    head_out = normalize(attended).astype(jnp.bfloat16).reshape(length, head_group * head_dim)
    merged = lax.all_to_all(head_out, "sp", split_axis=0, concat_axis=1, tiled=True)
    result = jnp.dot(
        merged,
        lax.all_gather(out_columns, "sp", axis=0, tiled=True),
        preferred_element_type=jnp.float32,
    )
    return result.astype(jnp.bfloat16)[None]


def solution(mesh):
    placed = (
        P("dp", "sp", None),
        P("dp", "sp"),
        P("dp", "sp"),
        P("dp", "sp"),
        P("sp", "dp"),
        P(),
        P("dp", "sp", None),
    )
    return jax.shard_map(
        on_device, mesh=mesh, in_specs=placed, out_specs=P("dp", "sp", None), check_vma=False
    )
```

profile of v0, /device:TPU:0, one launch (start us, length us, event | category | flops | bytes accessed | tf_op | source)
XLA Modules:
  0.0 412.7 jit_solution(10661305282785432766)
XLA Ops:
  11.3 9.1 %all_gather.14 = bf16[128,2048]{1,0:T(8,128)(2,1)} all-gather(bf16[128,512]{1,0:T(8,128)(2,1)S(1)} %copy-done.1), channel_id=1, replica_groups=mesh['sp'=8,'dp'=4] {'dp'}, dimensions={1}, use_global_device_ids=true | all-gather | bytes 655360 | tf_op jit(solution)/shard_map/all_gather | solution.py:67
  20.4 12.5 %all-gather.5.cloned.1.call-done = bf16[3,2048,128]{1,2,0:T(8,128)(2,1)} async-done(((bf16[3,512,128]{1,2,0:T(8,128)(2,1)}), bf16[3,2048,128]{1,2,0:T(8,128)(2,1)}) %all-gather.5.cloned.1.call-update) | async-done | bytes 1572880 | tf_op jit(solution)/shard_map/all_gather | solution.py:66
  33.0 152.7 %all-gather.9.cloned.1.call-done = bf16[1,2560,2048]{2,1,0:T(8,128)(2,1)} async-done(((bf16[1,320,2048]{2,1,0:T(8,128)(2,1)}), bf16[1,2560,2048]{2,1,0:T(8,128)(2,1)}) %all-gather.9.cloned.1.call-update) | async-done | bytes 10485776 | tf_op jit(solution)/shard_map/all_gather | solution.py:69
  185.7 8.7 %fusion.17 = bf16[3,2560,128]{1,2,0:T(8,128)(2,1)S(1)} fusion(bf16[3,2048,128]{1,2,0:T(8,128)(2,1)} %all-gather.5.cloned.1.call-done, bf16[1,2560,2048]{2,1,0:T(8,128)(2,1)} %all-gather.9.cloned.1.call-done), kind=kOutput, calls=%fused_computation.25 | convolution fusion | flops 4027514880 | bytes 14024704 | tf_op jit(solution)/shard_map/td,kdc->ktc/dot_general | solution.py:70
  195.3 176.2 %while.33 = (s32[]{:T(128)}, f32[5,512,2,64]{1,3,2,0:T(8,128)S(1)}, s32[5]{0:T(128)S(1)}, bf16[2560,2,64]{0,2,1:T(8,128)(2,1)S(1)}, f32[2,2560]{1,0:T(2,128)}, /...) while((s32[]{:T(128)}, f32[5,512,2,64]{1,3,2,0:T(8,128)S(1)}, ...), condition=%wide.region_9.10_spmd, body=%wide.region_2.9_spmd.sunk | while | flops 143990816 | bytes 31886096 | solution.py:55
  198.1 5.3 %broadcast.99 = f32[2,512,2560]{1,2,0:T(8,128)} broadcast(f32[]{:T(128)} %constant.14.clone.6..sunk), dimensions={} | broadcast | bytes 10485764 | tf_op jit(solution)/shard_map/broadcast.5
  203.4 2.9 while.34
  204.3 2.0 fusion.46
  206.3 13.8 %divide_convert_fusion.2 = bf16[2,512,2560]{1,2,0:T(8,128)(2,1)} fusion(f32[2,512,2560]{1,2,0:T(8,128)} %get-tuple-element.345), kind=kOutput, calls=%fused_computation.16.clone.1 | output fusion | flops 7871486 | bytes 15728640 | tf_op jit(solution)/shard_map/while/body/eval_jaxpr/div | solution.py:42
  220.2 1.6 while.35
  220.2 1.6 fusion.49
  224.4 5.3 %broadcast.99 = f32[2,512,2560]{1,2,0:T(8,128)} broadcast(f32[]{:T(128)} %constant.14.clone.6..sunk), dimensions={} | broadcast | bytes 10485764 | tf_op jit(solution)/shard_map/broadcast.5
  229.7 5.8 %while.34 = (s32[]{:T(128)}, f32[2,512,2560]{1,2,0:T(8,128)}, s32[]{:T(128)}, bf16[2560,2,64]{0,2,1:T(8,128)(2,1)S(1)}, bf16[512,2,64]{0,2,1:T(8,128)(2,1)S(1)},...) while((s32[]{:T(128)}, f32[2,512,2560]{1,2,0:T(8,128)}, ...), condition=%wide.region_4.4_spmd.clone, body=%wide.region_3.3_spmd.clone.sunk | while | flops 68944904 | bytes 2909359 | solution.py:39
  230.6 2.0 fusion.46
  233.5 1.9 fusion.46
  235.5 13.8 %divide_convert_fusion.2 = bf16[2,512,2560]{1,2,0:T(8,128)(2,1)} fusion(f32[2,512,2560]{1,2,0:T(8,128)} %get-tuple-element.345), kind=kOutput, calls=%fused_computation.16.clone.1 | output fusion | flops 7871486 | bytes 15728640 | tf_op jit(solution)/shard_map/while/body/eval_jaxpr/div | solution.py:42
  249.3 3.1 while.35
  255.1 5.3 %broadcast.99 = f32[2,512,2560]{1,2,0:T(8,128)} broadcast(f32[]{:T(128)} %constant.14.clone.6..sunk), dimensions={} | broadcast | bytes 10485764 | tf_op jit(solution)/shard_map/broadcast.5
  260.4 8.7 %while.34 = (s32[]{:T(128)}, f32[2,512,2560]{1,2,0:T(8,128)}, s32[]{:T(128)}, bf16[2560,2,64]{0,2,1:T(8,128)(2,1)S(1)}, bf16[512,2,64]{0,2,1:T(8,128)(2,1)S(1)},...) while((s32[]{:T(128)}, f32[2,512,2560]{1,2,0:T(8,128)}, ...), condition=%wide.region_4.4_spmd.clone, body=%wide.region_3.3_spmd.clone.sunk | while | flops 68944904 | bytes 2909359 | solution.py:39
  261.3 2.0 fusion.46
  264.2 1.9 fusion.46
  267.1 2.0 fusion.46
  269.1 13.8 %divide_convert_fusion.2 = bf16[2,512,2560]{1,2,0:T(8,128)(2,1)} fusion(f32[2,512,2560]{1,2,0:T(8,128)} %get-tuple-element.345), kind=kOutput, calls=%fused_computation.16.clone.1 | output fusion | flops 7871486 | bytes 15728640 | tf_op jit(solution)/shard_map/while/body/eval_jaxpr/div | solution.py:42
  282.9 4.7 %while.35 = (s32[]{:T(128)}, f32[512,2,64]{0,2,1:T(8,128)S(1)}, s32[]{:T(128)}, bf16[2560,2,64]{0,2,1:T(8,128)(2,1)S(1)}, bf16[2,512,2560]{1,2,0:T(8,128)(2,1)},...) while((s32[]{:T(128)}, f32[512,2,64]{0,2,1:T(8,128)S(1)}, s32[]{:T(128)}, ...), condition=%wide.region_8.8_spmd, body=%wide.region_7.7_spmd.sunk | while | flops 67174408 | bytes 1705099 | solution.py:53
  284.5 1.5 fusion.49
  290.3 5.3 %broadcast.99 = f32[2,512,2560]{1,2,0:T(8,128)} broadcast(f32[]{:T(128)} %constant.14.clone.6..sunk), dimensions={} | broadcast | bytes 10485764 | tf_op jit(solution)/shard_map/broadcast.5
  295.6 11.7 %while.34 = (s32[]{:T(128)}, f32[2,512,2560]{1,2,0:T(8,128)}, s32[]{:T(128)}, bf16[2560,2,64]{0,2,1:T(8,128)(2,1)S(1)}, bf16[512,2,64]{0,2,1:T(8,128)(2,1)S(1)},...) while((s32[]{:T(128)}, f32[2,512,2560]{1,2,0:T(8,128)}, ...), condition=%wide.region_4.4_spmd.clone, body=%wide.region_3.3_spmd.clone.sunk | while | flops 68944904 | bytes 2909359 | solution.py:39
  296.5 2.0 fusion.46
  299.4 1.9 fusion.46
  302.3 2.0 fusion.46
  305.2 2.1 fusion.46
  307.2 13.8 %divide_convert_fusion.2 = bf16[2,512,2560]{1,2,0:T(8,128)(2,1)} fusion(f32[2,512,2560]{1,2,0:T(8,128)} %get-tuple-element.345), kind=kOutput, calls=%fused_computation.16.clone.1 | output fusion | flops 7871486 | bytes 15728640 | tf_op jit(solution)/shard_map/while/body/eval_jaxpr/div | solution.py:42
  321.1 6.3 %while.35 = (s32[]{:T(128)}, f32[512,2,64]{0,2,1:T(8,128)S(1)}, s32[]{:T(128)}, bf16[2560,2,64]{0,2,1:T(8,128)(2,1)S(1)}, bf16[2,512,2560]{1,2,0:T(8,128)(2,1)},...) while((s32[]{:T(128)}, f32[512,2,64]{0,2,1:T(8,128)S(1)}, s32[]{:T(128)}, ...), condition=%wide.region_8.8_spmd, body=%wide.region_7.7_spmd.sunk | while | flops 67174408 | bytes 1705099 | solution.py:53
  330.0 5.3 %broadcast.99 = f32[2,512,2560]{1,2,0:T(8,128)} broadcast(f32[]{:T(128)} %constant.14.clone.6..sunk), dimensions={} | broadcast | bytes 10485764 | tf_op jit(solution)/shard_map/broadcast.5
  335.3 14.5 %while.34 = (s32[]{:T(128)}, f32[2,512,2560]{1,2,0:T(8,128)}, s32[]{:T(128)}, bf16[2560,2,64]{0,2,1:T(8,128)(2,1)S(1)}, bf16[512,2,64]{0,2,1:T(8,128)(2,1)S(1)},...) while((s32[]{:T(128)}, f32[2,512,2560]{1,2,0:T(8,128)}, ...), condition=%wide.region_4.4_spmd.clone, body=%wide.region_3.3_spmd.clone.sunk | while | flops 68944904 | bytes 2909359 | solution.py:39
  336.2 2.0 fusion.46
  339.1 1.9 fusion.46
  342.0 2.0 fusion.46
  344.9 2.1 fusion.46
  347.9 1.9 fusion.46
  349.8 13.8 %divide_convert_fusion.2 = bf16[2,512,2560]{1,2,0:T(8,128)(2,1)} fusion(f32[2,512,2560]{1,2,0:T(8,128)} %get-tuple-element.345), kind=kOutput, calls=%fused_computation.16.clone.1 | output fusion | flops 7871486 | bytes 15728640 | tf_op jit(solution)/shard_map/while/body/eval_jaxpr/div | solution.py:42
  363.7 7.8 %while.35 = (s32[]{:T(128)}, f32[512,2,64]{0,2,1:T(8,128)S(1)}, s32[]{:T(128)}, bf16[2560,2,64]{0,2,1:T(8,128)(2,1)S(1)}, bf16[2,512,2560]{1,2,0:T(8,128)(2,1)},...) while((s32[]{:T(128)}, f32[512,2,64]{0,2,1:T(8,128)S(1)}, s32[]{:T(128)}, ...), condition=%wide.region_8.8_spmd, body=%wide.region_7.7_spmd.sunk | while | flops 67174408 | bytes 1705099 | solution.py:53
  372.4 1.9 reshape.100
  375.7 1.7 mul.100
  378.5 2.4 copy.29
  380.8 3.5 all-to-all-start
  384.4 17.0 %all-to-all-done = bf16[8,320,128]{2,1,0:T(8,128)(2,1)S(1)} async-done(((bf16[8,320,128]{2,1,0:T(8,128)(2,1)}), bf16[8,320,128]{2,1,0:T(8,128)(2,1)S(1)}, u32[]{:S(2)}, u32[]{:S(2)}) %all-to-all-start) | async-done | bytes 655392 | tf_op jit(solution)/shard_map/all_to_all | solution.py:79
  401.4 4.8 %fusion.20 = bf16[1,320,2048]{2,1,0:T(8,128)(2,1)} fusion(bf16[1024,2048]{1,0:T(8,128)(2,1)} %all-gather.7.cloned.1.call-done, bf16[8,320,128]{2,1,0:T(8,128)(2,1)S(1)} %all-to-all-done), kind=kOutput, calls=%fused_computation.27 | convolution fusion | flops 1342832640 | bytes 6160384 | tf_op jit(solution)/shard_map/dot_general | solution.py:80
  (114 shorter events, 49.1 us)
Async XLA Ops:
  6.5 4.7 %copy-start.1 = (bf16[128,512]{1,0:T(8,128)(2,1)S(1)}, bf16[128,512]{1,0:T(8,128)(2,1)}, u32[]{:S(2)}) copy-start(bf16[128,512]{1,0:T(8,128)(2,1)} %param.17) | copy-start | bytes 393220
  6.5 26.4 %all-gather.5.cloned.1.call-start = ((), (), s32[]{:S(2)}) async-start(), calls=%async_computation.1 | async-start | bytes 1966080 | tf_op jit(solution)/shard_map/all_gather | solution.py:66
  8.6 11.8 %copy-start.2 = (f32[2,64]{1,0:T(2,128)S(1)}, f32[2,64]{1,0:T(2,128)}, u32[]{:S(2)}) copy-start(f32[2,64]{1,0:T(2,128)} %param.18) | copy-start | bytes 1540
  10.4 175.2 %all-gather.9.cloned.1.call-start = ((), (), s32[]{:S(2)}) async-start(), calls=%async_computation.3 | async-start | bytes 11796480 | tf_op jit(solution)/shard_map/all_gather | solution.py:69
  11.2 373.2 %all-gather.7.cloned.1.call-start = ((), (), s32[]{:S(2)}) async-start(), calls=%async_computation.2 | async-start | bytes 4718592 | tf_op jit(solution)/shard_map/all_gather | solution.py:82
  374.5 2.9 copy-start
  380.8 20.6 %all-to-all-start = ((bf16[8,320,128]{2,1,0:T(8,128)(2,1)}), bf16[8,320,128]{2,1,0:T(8,128)(2,1)S(1)}, u32[]{:S(2)}, u32[]{:S(2)}) async-start(bf16[8,320,128]{2,1,0:T(8,128)(2,1)} %copy.29), calls=%async_computation | async-start | bytes 1310720 | tf_op jit(solution)/shard_map/all_to_all | solution.py:79
Sparse Core Ops, SparseCore 0:
  10.6 22.3 all-gather.4
  35.1 150.5 all-gather.8
  187.8 70.9 all-gather.6
where the time goes:
time: 414 us; the launch traced here: 413 us
  waiting for transfers between devices  183 us (44%)
  other arithmetic  75.1 us (18%)
  matrix products  66.4 us (16%)
  local copies, waits for them, and re-layouts  54.8 us (13%)
  between operations  13.3 us (3%)
  blocking collectives  9.1 us (2%)
  loops' own time  7.36 us (2%)
    all_gather x1, waiting for transfers between devices, on_device(): whole = lax.all_gather(own_rows, 'sp', axis=0, tiled=True)  153 us
    div x5, other arithmetic, one_block(): weights / jnp.sum(weights, axis=-1, keepdims=True)  69 us
    dot_general x15, matrix products, fill(): jnp.einsum('qhd,khd->hqk', query_block, key_block, preferred_element_type...  29.8 us
    another operation x10, local copies, waits for them, and re-layouts  26.7 us
    dot_general x15, matrix products, gather_values(): jnp.einsum('hqk,khd->qhd', prob_block, value_block, preferred_element_typ...  23.1 us
    all_to_all x1, waiting for transfers between devices, on_device(): lax.all_to_all(head_out, 'sp', split_axis=0, concat_axis=1, tiled=True)  17 us
    all_gather x1, waiting for transfers between devices, on_device(): lax.all_gather(stacked, 'dp', axis=1, tiled=True)  12.5 us
    dynamic_slice x15, local copies, waits for them, and re-layouts, fill(): decay_keys = lax.dynamic_slice_in_dim(decay_rows, key_start, block, 1)  10.3 us
  transfers between devices with their start and end apart: 4, of which 3 were waited for; matrix products, arithmetic and copies ran while one was open for 45% of the time, Pallas kernels for 0%

commit v1 on v0

--- a/solution.py
+++ b/solution.py
@@ -2,6 +2,20 @@
 import jax.numpy as jnp
 from jax import lax
 from jax.sharding import PartitionSpec as P
+
+
+def work_both_ways(x, axis, dim, make, out_dim):
+    ways, here, step = (lax.axis_size(axis), lax.axis_index(axis), x.shape[dim])
+    earlier, later = ([], [])
+    going_up = going_down = x
+    for far in range(ways // 2 + 1):
+        earlier.append(make(going_up, (here - far) % ways * step))
+        if 0 < far < ways - ways // 2:
+            later.append(make(going_down, (here + far) % ways * step))
+        going_up = lax.ppermute(going_up, axis, [(d, (d + 1) % ways) for d in range(ways)])
+        going_down = lax.ppermute(going_down, axis, [(d, (d - 1) % ways) for d in range(ways)])
+    line = jnp.concatenate([*earlier[::-1], *later], axis=out_dim)
+    return jnp.roll(line, (here - ways // 2) * earlier[0].shape[out_dim], axis=out_dim)
 
 
 def normalize(values):
@@ -66,10 +80,15 @@
         lax.all_gather(stacked, "dp", axis=1, tiled=True),
         lax.all_gather(w_output, "dp", axis=1, tiled=True),
     )
-    whole = lax.all_gather(own_rows, "sp", axis=0, tiled=True)
-    triple = jnp.einsum("td,kdc->ktc", whole, columns, preferred_element_type=jnp.float32).astype(
-        jnp.bfloat16
-    )
+    triple = work_both_ways(
+        own_rows,
+        "sp",
+        0,
+        lambda shard, at: jnp.einsum(
+            "td,kdc->ktc", shard, columns, preferred_element_type=jnp.float32
+        ),
+        1,
+    ).astype(jnp.bfloat16)
     length = triple.shape[1]
     grouped = triple.reshape(3, length, head_group, head_dim)
     query_unit = (normalize(grouped[0]) * qk_gain[0] * head_dim ** (-0.5)).astype(jnp.bfloat16)

time: 414 us -> 493 us (1.19)
  starting transfers between devices: 3.62 us -> 67.6 us
  waiting for transfers between devices: 183 us -> 145 us
  matrix products: 66.4 us -> 86.2 us
  blocking collectives: 9.1 us -> 27.5 us
  local copies, waits for them, and re-layouts: 54.8 us -> 65.2 us
    all_gather x1 -> x0, waiting for transfers between devices: 153 us -> none  [on_device(): whole = lax.all_gather(own_rows, 'sp', axis=0, tiled=True)]
    ppermute x0 -> x7, waiting for transfers between devices: none -> 145 us  [the longest x4 134 us: work_both_ways(): lax.ppermute(going_up, axis, [(d, (d + 1) % ways) for d in range(ways)])]
    ppermute x0 -> x7, starting transfers between devices: none -> 67.6 us  [the longest x3 59.5 us: work_both_ways(): lax.ppermute(going_down, axis, [(d, (d - 1) % ways) for d in range(ways)])]
    all_to_all x0 -> x1, blocking collectives: none -> 19.6 us  [on_device(): lax.all_to_all(head_out, 'sp', split_axis=0, concat_axis=1, tiled=True)]
    all_to_all x1 -> x0, waiting for transfers between devices: 17 us -> none  [on_device(): lax.all_to_all(head_out, 'sp', split_axis=0, concat_axis=1, tiled=True)]
    dot_general x15, matrix products: 29.8 us -> 43.6 us  [fill(): jnp.einsum('qhd,khd->hqk', query_block, key_block, preferred_element_type...]
    all_gather x1, waiting for transfers between devices: 12.5 us -> 0.01 us  [on_device(): lax.all_gather(stacked, 'dp', axis=1, tiled=True)]
    dot_general x1 -> x8, matrix products: 8.71 us -> 14.7 us  [on_device(): jnp.einsum('td,kdc->ktc', shard, columns, preferred_element_type=jnp.floa...]
  transfers between devices with their start and end apart: 4 -> 9, of which waited for: 3 -> 5; matrix products, arithmetic and copies ran while one was open for 45% -> 46% of each run, Pallas kernels for 0% -> 0%
where the time goes in v1:
time: 493 us; the launch traced here: 491 us
  waiting for transfers between devices  145 us (29%)
  matrix products  86.2 us (17%)
  other arithmetic  79.4 us (16%)
  starting transfers between devices  67.6 us (14%)
  local copies, waits for them, and re-layouts  65.2 us (13%)
  blocking collectives  27.5 us (6%)
  between operations  13.7 us (3%)
  loops' own time  6.89 us (1%)
    ppermute x4, waiting for transfers between devices, work_both_ways(): lax.ppermute(going_up, axis, [(d, (d + 1) % ways) for d in range(ways)])  134 us
    div x5, other arithmetic, one_block(): weights / jnp.sum(weights, axis=-1, keepdims=True)  69.8 us
    ppermute x3, starting transfers between devices, work_both_ways(): lax.ppermute(going_down, axis, [(d, (d - 1) % ways) for d in range(ways)])  59.5 us
    dot_general x15, matrix products, fill(): jnp.einsum('qhd,khd->hqk', query_block, key_block, preferred_element_type...  43.6 us
    another operation x10, local copies, waits for them, and re-layouts  26.8 us
    dot_general x15, matrix products, gather_values(): jnp.einsum('hqk,khd->qhd', prob_block, value_block, preferred_element_typ...  23.1 us
    all_to_all x1, blocking collectives, on_device(): lax.all_to_all(head_out, 'sp', split_axis=0, concat_axis=1, tiled=True)  19.6 us
    dot_general x8, matrix products, on_device(): jnp.einsum('td,kdc->ktc', shard, columns, preferred_element_type=jnp.floa...  14.7 us
  transfers between devices with their start and end apart: 9, of which 5 were waited for; matrix products, arithmetic and copies ran while one was open for 46% of the time, Pallas kernels for 0%

profile of v1, /device:TPU:0, one launch (start us, length us, event | category | flops | bytes accessed | tf_op | source)
XLA Modules:
  0.0 491.1 jit_solution(16437094259261234924)
XLA Ops:
  6.5 3.0 collective-permute-start
  9.5 32.0 %collective-permute-done = bf16[320,2048]{1,0:T(8,128)(2,1)S(1)} collective-permute-done((bf16[320,2048]{1,0:T(8,128)(2,1)}, bf16[320,2048]{1,0:T(8,128)(2,1)S(1)}, u32[]{:S(2)}, u32[]{:S(2)}) %collective-permute-start) | collective-permute-done | bytes 1310752 | tf_op jit(solution)/shard_map/ppermute | solution.py:15
  41.6 4.7 collective-permute-start.4
  46.3 51.1 %collective-permute-done.1 = bf16[320,2048]{1,0:T(8,128)(2,1)} collective-permute-done((bf16[320,2048]{1,0:T(8,128)(2,1)S(1)}, bf16[320,2048]{1,0:T(8,128)(2,1)}, u32[]{:S(2)}, u32[]{:S(2)}) %collective-permute-start.1) | collective-permute-done | bytes 1310752 | tf_op jit(solution)/shard_map/ppermute | solution.py:15
  101.9 27.2 %collective-permute-start.5 = (bf16[320,2048]{1,0:T(8,128)(2,1)S(1)}, bf16[320,2048]{1,0:T(8,128)(2,1)}, u32[]{:S(2)}, u32[]{:S(2)}) collective-permute-start(bf16[320,2048]{1,0:T(8,128)(2,1)S(1)} %collective-permute-done.4), channel_id=1, source_target_pairs={{0,28},{4,0},{8,4},{12,8},{16,12},{20,16},{24,20},{28,24},{1,29},{... | collective-permute-start | bytes 3932168 | tf_op jit(solution)/shard_map/ppermute | solution.py:16
  129.1 26.2 %collective-permute-done.2 = bf16[320,2048]{1,0:T(8,128)(2,1)} collective-permute-done((bf16[320,2048]{1,0:T(8,128)(2,1)}, bf16[320,2048]{1,0:T(8,128)(2,1)}, u32[]{:S(2)}, u32[]{:S(2)}) %collective-permute-start.2) | collective-permute-done | bytes 1310752 | tf_op jit(solution)/shard_map/ppermute | solution.py:15
  157.8 7.9 %all_gather.10 = bf16[128,2048]{1,0:T(8,128)(2,1)} all-gather(bf16[128,512]{1,0:T(8,128)(2,1)} %param.17), channel_id=1, replica_groups=mesh['sp'=8,'dp'=4] {'dp'}, dimensions={1}, use_global_device_ids=true | all-gather | bytes 655360 | tf_op jit(solution)/shard_map/all_gather | solution.py:81
  165.7 27.7 %collective-permute-start.6 = (bf16[320,2048]{1,0:T(8,128)(2,1)}, bf16[320,2048]{1,0:T(8,128)(2,1)}, u32[]{:S(2)}, u32[]{:S(2)}) collective-permute-start(bf16[320,2048]{1,0:T(8,128)(2,1)} %collective-permute-done.5), channel_id=1, source_target_pairs={{0,28},{4,0},{8,4},{12,8},{16,12},{20,16},{24,20},{28,24},{1,29},{... | collective-permute-start | bytes 3932168 | tf_op jit(solution)/shard_map/ppermute | solution.py:16
  193.4 24.4 %collective-permute-done.3 = bf16[320,2048]{1,0:T(8,128)(2,1)} collective-permute-done((bf16[320,2048]{1,0:T(8,128)(2,1)}, bf16[320,2048]{1,0:T(8,128)(2,1)}, u32[]{:S(2)}, u32[]{:S(2)}) %collective-permute-start.3) | collective-permute-done | bytes 1310752 | tf_op jit(solution)/shard_map/ppermute | solution.py:15
  217.8 3.0 constant_dynamic-update-slice_fusion.15
  230.7 10.8 %collective-permute-done.6 = bf16[320,2048]{1,0:T(8,128)(2,1)} collective-permute-done((bf16[320,2048]{1,0:T(8,128)(2,1)}, bf16[320,2048]{1,0:T(8,128)(2,1)}, u32[]{:S(2)}, u32[]{:S(2)}) %collective-permute-start.6) | collective-permute-done | bytes 1310752 | tf_op jit(solution)/shard_map/ppermute | solution.py:16
  251.3 198.5 %while.33 = (s32[]{:T(128)}, f32[5,512,2,64]{1,3,2,0:T(8,128)}, s32[5]{0:T(128)S(1)}, bf16[2560,2,64]{0,2,1:T(8,128)(2,1)}, f32[2,2560]{1,0:T(2,128)}, /*index=5...) while((s32[]{:T(128)}, f32[5,512,2,64]{1,3,2,0:T(8,128)}, ...), condition=%wide.region_9.10_spmd, body=%wide.region_2.9_spmd.sunk | while | flops 143990816 | bytes 31886604 | solution.py:69
  254.8 5.3 %broadcast.99 = f32[2,512,2560]{1,2,0:T(8,128)} broadcast(f32[]{:T(128)} %constant.56.clone.6..sunk), dimensions={} | broadcast | bytes 10485764 | tf_op jit(solution)/shard_map/broadcast.5
  260.1 3.8 while.34
  261.1 2.9 fusion.78
  264.0 14.0 %divide_convert_fusion.2 = bf16[2,512,2560]{1,2,0:T(8,128)(2,1)} fusion(f32[2,512,2560]{1,2,0:T(8,128)} %get-tuple-element.368), kind=kOutput, calls=%fused_computation.16.clone.1 | output fusion | flops 7871486 | bytes 15728640 | tf_op jit(solution)/shard_map/while/body/eval_jaxpr/div | solution.py:56
  283.7 5.3 %broadcast.99 = f32[2,512,2560]{1,2,0:T(8,128)} broadcast(f32[]{:T(128)} %constant.56.clone.6..sunk), dimensions={} | broadcast | bytes 10485764 | tf_op jit(solution)/shard_map/broadcast.5
  289.1 7.6 %while.34 = (s32[]{:T(128)}, f32[2,512,2560]{1,2,0:T(8,128)}, s32[]{:T(128)}, bf16[2560,2,64]{0,2,1:T(8,128)(2,1)}, bf16[512,2,64]{0,2,1:T(8,128)(2,1)S(1)}, /*i...) while((s32[]{:T(128)}, f32[2,512,2560]{1,2,0:T(8,128)}, ...), condition=%wide.region_4.4_spmd.clone, body=%wide.region_3.3_spmd.clone.sunk | while | flops 68944904 | bytes 2909359 | solution.py:53
  290.0 2.9 fusion.78
  293.8 2.9 fusion.78
  296.7 14.0 %divide_convert_fusion.2 = bf16[2,512,2560]{1,2,0:T(8,128)(2,1)} fusion(f32[2,512,2560]{1,2,0:T(8,128)} %get-tuple-element.368), kind=kOutput, calls=%fused_computation.16.clone.1 | output fusion | flops 7871486 | bytes 15728640 | tf_op jit(solution)/shard_map/while/body/eval_jaxpr/div | solution.py:56
  310.7 3.1 while.35
  318.0 5.3 %broadcast.99 = f32[2,512,2560]{1,2,0:T(8,128)} broadcast(f32[]{:T(128)} %constant.56.clone.6..sunk), dimensions={} | broadcast | bytes 10485764 | tf_op jit(solution)/shard_map/broadcast.5
  323.3 11.5 %while.34 = (s32[]{:T(128)}, f32[2,512,2560]{1,2,0:T(8,128)}, s32[]{:T(128)}, bf16[2560,2,64]{0,2,1:T(8,128)(2,1)}, bf16[512,2,64]{0,2,1:T(8,128)(2,1)S(1)}, /*i...) while((s32[]{:T(128)}, f32[2,512,2560]{1,2,0:T(8,128)}, ...), condition=%wide.region_4.4_spmd.clone, body=%wide.region_3.3_spmd.clone.sunk | while | flops 68944904 | bytes 2909359 | solution.py:53
  324.3 2.9 fusion.78
  328.1 2.9 fusion.78
  331.9 2.9 fusion.78
  334.8 14.0 %divide_convert_fusion.2 = bf16[2,512,2560]{1,2,0:T(8,128)(2,1)} fusion(f32[2,512,2560]{1,2,0:T(8,128)} %get-tuple-element.368), kind=kOutput, calls=%fused_computation.16.clone.1 | output fusion | flops 7871486 | bytes 15728640 | tf_op jit(solution)/shard_map/while/body/eval_jaxpr/div | solution.py:56
  348.8 4.7 while.35
  357.7 5.3 %broadcast.99 = f32[2,512,2560]{1,2,0:T(8,128)} broadcast(f32[]{:T(128)} %constant.56.clone.6..sunk), dimensions={} | broadcast | bytes 10485764 | tf_op jit(solution)/shard_map/broadcast.5
  363.0 15.4 %while.34 = (s32[]{:T(128)}, f32[2,512,2560]{1,2,0:T(8,128)}, s32[]{:T(128)}, bf16[2560,2,64]{0,2,1:T(8,128)(2,1)}, bf16[512,2,64]{0,2,1:T(8,128)(2,1)S(1)}, /*i...) while((s32[]{:T(128)}, f32[2,512,2560]{1,2,0:T(8,128)}, ...), condition=%wide.region_4.4_spmd.clone, body=%wide.region_3.3_spmd.clone.sunk | while | flops 68944904 | bytes 2909359 | solution.py:53
  364.0 2.9 fusion.78
  367.8 2.9 fusion.78
  371.6 2.9 fusion.78
  375.4 3.0 fusion.78
  378.4 14.0 %divide_convert_fusion.2 = bf16[2,512,2560]{1,2,0:T(8,128)(2,1)} fusion(f32[2,512,2560]{1,2,0:T(8,128)} %get-tuple-element.368), kind=kOutput, calls=%fused_computation.16.clone.1 | output fusion | flops 7871486 | bytes 15728640 | tf_op jit(solution)/shard_map/while/body/eval_jaxpr/div | solution.py:56
  392.4 6.3 %while.35 = (s32[]{:T(128)}, f32[512,2,64]{0,2,1:T(8,128)S(1)}, s32[]{:T(128)}, bf16[2560,2,64]{0,2,1:T(8,128)(2,1)S(1)}, bf16[2,512,2560]{1,2,0:T(8,128)(2,1)},...) while((s32[]{:T(128)}, f32[512,2,64]{0,2,1:T(8,128)S(1)}, s32[]{:T(128)}, ...), condition=%wide.region_8.8_spmd, body=%wide.region_7.7_spmd.sunk | while | flops 67174408 | bytes 1705099 | solution.py:67
  402.9 5.3 %broadcast.99 = f32[2,512,2560]{1,2,0:T(8,128)} broadcast(f32[]{:T(128)} %constant.56.clone.6..sunk), dimensions={} | broadcast | bytes 10485764 | tf_op jit(solution)/shard_map/broadcast.5
  408.2 19.1 %while.34 = (s32[]{:T(128)}, f32[2,512,2560]{1,2,0:T(8,128)}, s32[]{:T(128)}, bf16[2560,2,64]{0,2,1:T(8,128)(2,1)}, bf16[512,2,64]{0,2,1:T(8,128)(2,1)S(1)}, /*i...) while((s32[]{:T(128)}, f32[2,512,2560]{1,2,0:T(8,128)}, ...), condition=%wide.region_4.4_spmd.clone, body=%wide.region_3.3_spmd.clone.sunk | while | flops 68944904 | bytes 2909359 | solution.py:53
  409.1 2.9 fusion.78
  412.9 2.9 fusion.78
  416.7 2.9 fusion.78
  420.6 3.0 fusion.78
  424.5 2.8 fusion.78
  427.3 14.0 %divide_convert_fusion.2 = bf16[2,512,2560]{1,2,0:T(8,128)(2,1)} fusion(f32[2,512,2560]{1,2,0:T(8,128)} %get-tuple-element.368), kind=kOutput, calls=%fused_computation.16.clone.1 | output fusion | flops 7871486 | bytes 15728640 | tf_op jit(solution)/shard_map/while/body/eval_jaxpr/div | solution.py:56
  441.3 7.9 %while.35 = (s32[]{:T(128)}, f32[512,2,64]{0,2,1:T(8,128)S(1)}, s32[]{:T(128)}, bf16[2560,2,64]{0,2,1:T(8,128)(2,1)S(1)}, bf16[2,512,2560]{1,2,0:T(8,128)(2,1)},...) while((s32[]{:T(128)}, f32[512,2,64]{0,2,1:T(8,128)S(1)}, s32[]{:T(128)}, ...), condition=%wide.region_8.8_spmd, body=%wide.region_7.7_spmd.sunk | while | flops 67174408 | bytes 1705099 | solution.py:67
  459.8 19.6 %all_to_all.16 = bf16[8,320,128]{2,1,0:T(8,128)(2,1)S(1)} all-to-all(bf16[8,320,128]{2,1,0:T(8,128)(2,1)S(1)} %copy.29), channel_id=1, replica_groups=mesh['sp'=8,'dp'=4] {'sp'}, dimensions={0} | all-to-all | bytes 1310720 | tf_op jit(solution)/shard_map/all_to_all | solution.py:98
  479.5 4.8 fusion.12
  (144 shorter events, 89.4 us)
Async XLA Ops:
  6.5 159.2 %copy-start.2 = (f32[2,64]{1,0:T(2,128)S(1)}, f32[2,64]{1,0:T(2,128)}, u32[]{:S(2)}) copy-start(f32[2,64]{1,0:T(2,128)} %param.18) | copy-start | bytes 1540
  6.5 186.8 %all-gather.3.cloned.1.call-start = ((), (), s32[]{:S(2)}) async-start(), calls=%async_computation.1 | async-start | bytes 1966080 | tf_op jit(solution)/shard_map/all_gather | solution.py:80
  6.5 35.0 %collective-permute-start = (bf16[320,2048]{1,0:T(8,128)(2,1)}, bf16[320,2048]{1,0:T(8,128)(2,1)S(1)}, u32[]{:S(2)}, u32[]{:S(2)}) collective-permute-start(bf16[320,2048]{1,0:T(8,128)(2,1)} %bitcast.146), channel_id=1, source_target_pairs={{0,4},{4,8},{8,12},{12,16},{16,20},{20,24},{24,28},{28,0},{1,5},{5... | collective-permute-start | bytes 3932168 | tf_op jit(solution)/shard_map/ppermute | solution.py:15
  41.6 55.8 %collective-permute-start.1 = (bf16[320,2048]{1,0:T(8,128)(2,1)S(1)}, bf16[320,2048]{1,0:T(8,128)(2,1)}, u32[]{:S(2)}, u32[]{:S(2)}) collective-permute-start(bf16[320,2048]{1,0:T(8,128)(2,1)S(1)} %collective-permute-done), channel_id=1, source_target_pairs={{0,4},{4,8},{8,12},{12,16},{16,20},{20,24},{24,28},{28,0},{1,5},{5... | collective-permute-start | bytes 3932168 | tf_op jit(solution)/shard_map/ppermute | solution.py:15
  41.6 60.3 %collective-permute-start.4 = (bf16[320,2048]{1,0:T(8,128)(2,1)}, bf16[320,2048]{1,0:T(8,128)(2,1)S(1)}, u32[]{:S(2)}, u32[]{:S(2)}) collective-permute-start(bf16[320,2048]{1,0:T(8,128)(2,1)} %bitcast.147), channel_id=1, source_target_pairs={{0,28},{4,0},{8,4},{12,8},{16,12},{20,16},{24,20},{28,24},{1,29},{... | collective-permute-start | bytes 3932168 | tf_op jit(solution)/shard_map/ppermute | solution.py:16
  97.4 57.9 %collective-permute-start.2 = (bf16[320,2048]{1,0:T(8,128)(2,1)}, bf16[320,2048]{1,0:T(8,128)(2,1)}, u32[]{:S(2)}, u32[]{:S(2)}) collective-permute-start(bf16[320,2048]{1,0:T(8,128)(2,1)} %collective-permute-done.1), channel_id=1, source_target_pairs={{0,4},{4,8},{8,12},{12,16},{16,20},{20,24},{24,28},{28,0},{1,5},{5... | collective-permute-start | bytes 3932168 | tf_op jit(solution)/shard_map/ppermute | solution.py:15
  101.8 377.6 %all-gather.5.cloned.1.call-start = ((), (), s32[]{:S(2)}) async-start(), calls=%async_computation.2 | async-start | bytes 4718592 | tf_op jit(solution)/shard_map/all_gather | solution.py:101
  101.9 63.8 %collective-permute-start.5 = (bf16[320,2048]{1,0:T(8,128)(2,1)S(1)}, bf16[320,2048]{1,0:T(8,128)(2,1)}, u32[]{:S(2)}, u32[]{:S(2)}) collective-permute-start(bf16[320,2048]{1,0:T(8,128)(2,1)S(1)} %collective-permute-done.4), channel_id=1, source_target_pairs={{0,28},{4,0},{8,4},{12,8},{16,12},{20,16},{24,20},{28,24},{1,29},{... | collective-permute-start | bytes 3932168 | tf_op jit(solution)/shard_map/ppermute | solution.py:16
  155.3 62.5 %collective-permute-start.3 = (bf16[320,2048]{1,0:T(8,128)(2,1)}, bf16[320,2048]{1,0:T(8,128)(2,1)}, u32[]{:S(2)}, u32[]{:S(2)}) collective-permute-start(bf16[320,2048]{1,0:T(8,128)(2,1)} %collective-permute-done.2), channel_id=1, source_target_pairs={{0,4},{4,8},{8,12},{12,16},{16,20},{20,24},{24,28},{28,0},{1,5},{5... | collective-permute-start | bytes 3932168 | tf_op jit(solution)/shard_map/ppermute | solution.py:15
  165.7 75.8 %collective-permute-start.6 = (bf16[320,2048]{1,0:T(8,128)(2,1)}, bf16[320,2048]{1,0:T(8,128)(2,1)}, u32[]{:S(2)}, u32[]{:S(2)}) collective-permute-start(bf16[320,2048]{1,0:T(8,128)(2,1)} %collective-permute-done.5), channel_id=1, source_target_pairs={{0,28},{4,0},{8,4},{12,8},{16,12},{20,16},{24,20},{28,24},{1,29},{... | collective-permute-start | bytes 3932168 | tf_op jit(solution)/shard_map/ppermute | solution.py:16
  193.4 27.5 %copy-start.3 = (bf16[3,2048,128]{2,1,0:T(8,128)(2,1)S(1)}, bf16[3,2048,128]{2,1,0:T(8,128)(2,1)}, u32[]{:S(2)}) copy-start(bf16[3,2048,128]{2,1,0:T(8,128)(2,1)} %all-gather.3.cloned.1.call-done) | copy-start | bytes 4718596
  225.3 1.3 copy-start.4
  452.0 2.0 copy-start.1
  455.4 1.8 copy-start
Sparse Core Ops, SparseCore 0:
  102.0 18.2 all-gather.2
  165.8 97.7 all-gather.4
